TPU v7x, 32 devices: a whole 2x2x4 slice. The times are simulated.
32 devices in a mesh: sp: 8 (over z, y), tp: 4 (over x, core).
Axes of the slice: x: 2, y: 2, z: 4, core: 2. Of those that a mesh axis runs over, the one named last changes fastest.
Arguments:
- inputs: bfloat16 [8, 6144, 2048], P(None, ('sp', 'tp')), may hold values from -6 to 6
- norm_gain: bfloat16 [2048], replicated, may hold values from 0.099609375 to 1.8984375
- key_weight: bfloat16 [2048, 512], replicated, may hold values from -0.125 to 0.125
- value_weight: bfloat16 [2048, 512], replicated, may hold values from -0.125 to 0.125
- query: bfloat16 [8, 1024], P('sp', 'tp'), may hold values from -15 to 15
- head_bias: bfloat16 [16], P('tp'), may hold values from -14 to -6
Outputs:
- key_cache: bfloat16 [8, 6144, 512], P('sp', None, 'tp')
- value_cache: bfloat16 [8, 6144, 512], P('sp', None, 'tp')
- first_read: bfloat16 [8, 1024], P('sp', 'tp')
All inputs are finite; a program needn't handle non-finite values.
Results may differ from a plain program's by a relative error of at most 0.012.
Values may be sent and summed in bfloat16 or wider, within the bound.
A program may use at most 128 MiB of HBM per device.

v0:
```python
import jax
import jax.numpy as jnp
from jax import lax
from jax.sharding import PartitionSpec as P

HEAD_DIMENSION = 64


EPSILON = 1e-06


def body(inputs, norm_gain, key_weight, value_weight, query, head_bias):
    groups = lax.axis_size("tp")
    seq_count, span_len, model_width = inputs.shape
    head_cols = key_weight.shape[1] // groups
    kv_heads = head_cols // HEAD_DIMENSION
    q_heads = query.shape[1] // HEAD_DIMENSION
    repeat = q_heads // kv_heads
    widened = inputs.astype(jnp.float32)
    normed = widened * lax.rsqrt(jnp.mean(widened * widened, axis=-1, keepdims=True) + EPSILON)
    normed = (normed * norm_gain.astype(jnp.float32)).astype(jnp.bfloat16)
    key_rows = jnp.einsum(
        "kru,uao->karo",
        normed,
        key_weight.reshape(model_width, groups, head_cols),
        preferred_element_type=jnp.float32,
    ).astype(jnp.bfloat16)
    value_rows = jnp.einsum(
        "kru,uao->karo",
        normed,
        value_weight.reshape(model_width, groups, head_cols),
        preferred_element_type=jnp.float32,
    ).astype(jnp.bfloat16)
    key_cache, value_cache = (
        lax.all_to_all(
            key_rows.reshape(seq_count * groups, span_len, head_cols),
            ("sp", "tp"),
            split_axis=0,
            concat_axis=1,
            tiled=True,
        ),
        lax.all_to_all(
            value_rows.reshape(seq_count * groups, span_len, head_cols),
            ("sp", "tp"),
            split_axis=0,
            concat_axis=1,
            tiled=True,
        ),
    )
    seq_len = key_cache.shape[1]
    query_tensor = query.reshape(kv_heads, repeat, HEAD_DIMENSION)
    key_tensor = key_cache.reshape(seq_len, kv_heads, HEAD_DIMENSION)
    value_tensor = value_cache.reshape(seq_len, kv_heads, HEAD_DIMENSION)
    score_logits = jnp.einsum(
        "ebx,uex->ebu", query_tensor, key_tensor, preferred_element_type=jnp.float32
    )
    score_logits = score_logits * HEAD_DIMENSION ** (-0.5) + head_bias.astype(jnp.float32).reshape(
        kv_heads, repeat, 1
    )
    log_keep = jax.nn.log_sigmoid(-score_logits)
    suffix_logs = lax.cumsum(log_keep, axis=2, reverse=True) - log_keep
    stick_weights = jnp.exp(jax.nn.log_sigmoid(score_logits) + suffix_logs).astype(jnp.bfloat16)
    attended_output = jnp.einsum(
        "euq,qec->euc", stick_weights, value_tensor, preferred_element_type=jnp.float32
    )
    first_read = attended_output.reshape(1, q_heads * HEAD_DIMENSION).astype(jnp.bfloat16)
    return (key_cache, value_cache, first_read)


def solution(mesh):
    placed = (P(None, ("sp", "tp"), None), P(), P(), P(), P("sp", "tp"), P("tp"))
    return jax.shard_map(
        body,
        mesh=mesh,
        in_specs=placed,
        out_specs=(P("sp", None, "tp"), P("sp", None, "tp"), P("sp", "tp")),
        check_vma=False,
    )
```

profile of v0, /device:TPU:0, one launch (start us, length us, event | category | flops | bytes accessed | tf_op | source)
XLA Modules:
  0.0 114.2 jit_solution(8614409717820748399)
XLA Ops:
  0.6 0.0 copy-start
  0.6 0.0 copy-start.1
  0.7 0.0 copy-start.2
  0.7 4.2 %fusion = f32[8,192]{1,0:T(8,128)S(1)} fusion(bf16[8,192,2048]{2,1,0:T(8,128)(2,1)} %param.6), kind=kLoop, calls=%fused_computation.2 | loop fusion | flops 9435648 | bytes 6297600 | tf_op jit(solution)/shard_map/reduce_sum | solution.py:20
  4.9 0.0 copy-done.2
  4.9 0.0 copy-done
  5.0 0.9 copy-done.1
  5.9 4.6 %fusion.12 = bf16[8,192,4,128]{3,1,2,0:T(8,128)(2,1)} fusion(bf16[8,192,2048]{2,1,0:T(8,128)(2,1)S(1)} %copy-done.1, f32[2048]{0:T(1024)S(1)} %convert_element_type.40, f32[8,192]{1,0:T(8,128)S(1)} %add_rsqrt_fusion, bf16[2048,512]{1,0:T(8,128)(2,1)S(1)} %copy-done), kind=kOutput, calls=%fused_computation.15 | convolution fusion | flops 3234594816 | bytes 9975808 | tf_op jit(solution)/shard_map/kru,uao->karo/dot_general | solution.py:22
  10.5 7.4 %all-to-all-start = ((bf16[32,192,128]{2,1,0:T(8,128)(2,1)}), bf16[32,192,128]{2,1,0:T(8,128)(2,1)}, u32[]{:S(2)}, u32[]{:S(2)}) async-start(bf16[32,192,128]{2,1,0:T(8,128)(2,1)} %bitcast.58), calls=%async_computation | async-start | bytes 3145728 | tf_op jit(solution)/shard_map/all_to_all | solution.py:35
  17.9 8.2 %fusion.15 = bf16[8,192,4,128]{3,1,2,0:T(8,128)(2,1)} fusion(bf16[8,192,2048]{2,1,0:T(8,128)(2,1)} %param.6, f32[2048]{0:T(1024)S(1)} %convert_element_type.40, f32[8,192]{1,0:T(8,128)S(1)} %add_rsqrt_fusion, bf16[2048,512]{1,0:T(8,128)(2,1)} %param.9), kind=kOutput, calls=%fused_computation.16 | convolution fusion | flops 3234594816 | bytes 9975808 | tf_op jit(solution)/shard_map/kru,uao->karo/dot_general | solution.py:28
  26.1 0.0 copy-start.3
  26.1 0.0 copy-start.4
  26.1 29.4 %all-to-all-done = bf16[32,192,128]{2,1,0:T(8,128)(2,1)} async-done(((bf16[32,192,128]{2,1,0:T(8,128)(2,1)}), bf16[32,192,128]{2,1,0:T(8,128)(2,1)}, u32[]{:S(2)}, u32[]{:S(2)}) %all-to-all-start) | async-done | bytes 1572896 | tf_op jit(solution)/shard_map/all_to_all | solution.py:35
  55.6 4.1 %all-to-all-start.1 = ((bf16[32,192,128]{2,1,0:T(8,128)(2,1)}), bf16[32,192,128]{2,1,0:T(8,128)(2,1)}, u32[]{:S(2)}, u32[]{:S(2)}) async-start(bf16[32,192,128]{2,1,0:T(8,128)(2,1)} %bitcast.57), calls=%async_computation.1 | async-start | bytes 3145728 | tf_op jit(solution)/shard_map/all_to_all | solution.py:42
  59.7 0.0 copy-done.3
  59.7 0.1 reshape.75
  59.8 0.0 copy-done.4
  59.8 0.1 reshape.79
  59.9 4.5 %copy.21 = bf16[32,192,128]{1,0,2:T(8,128)(2,1)} copy(bf16[32,192,128]{2,1,0:T(8,128)(2,1)} %all-to-all-done) | data formatting | bytes 3145728 | tf_op jit(solution)/shard_map/all_to_all | solution.py:35
  64.4 4.5 %reshape.74 = bf16[6144,2,64]{0,2,1:T(8,128)(2,1)} reshape(bf16[32,192,128]{1,0,2:T(8,128)(2,1)} %copy.21) | data formatting | bytes 3145728 | tf_op jit(solution)/shard_map/reshape | solution.py:52
  68.9 1.8 %fusion.21 = (f32[2,2,6144]{2,1,0:T(2,128)S(1)}, f32[2,2,6144]{2,1,0:T(2,128)S(1)}) fusion(f32[2,2]{1,0:T(2,128)S(1)} %reshape.79, bf16[6144,2,64]{0,2,1:T(8,128)(2,1)} %reshape.74, bf16[2,2,64]{2,1,0:T(2,128)(2,1)S(1)} %reshape.75), kind=kOutput, calls=%fused_computation.23 | convolution fusion | flops 3366912 | bytes 1770000 | tf_op jit(solution)/shard_map/ebx,uex->ebu/dot_general | solution.py:54
  70.7 0.1 reshape.76
  70.8 5.0 %reduce-window.6 = f32[2,2,48,128]{3,2,1,0:T(8,128)S(1)} reduce-window(f32[2,2,48,128]{3,2,1,0:T(8,128)S(1)} %reshape.76, f32[]{:T(128)} %constant.6.clone.1), window={size=1x1x1x128 pad=0_0x0_0x0_0x0_127}, to_apply=%region_1.2 | reduce-window | flops 3121152 | bytes 196612 | tf_op jit(solution)/shard_map/reduce-window
  75.9 0.1 slice_reduce_fusion
  76.0 0.7 reduce-window.9
  76.6 0.1 slice.9
  76.7 0.1 broadcast_add_fusion
  76.8 0.1 reduce_window_sum.15
  76.9 20.3 %all-to-all-done.1 = bf16[32,192,128]{2,1,0:T(8,128)(2,1)} async-done(((bf16[32,192,128]{2,1,0:T(8,128)(2,1)}), bf16[32,192,128]{2,1,0:T(8,128)(2,1)}, u32[]{:S(2)}, u32[]{:S(2)}) %all-to-all-start.1) | async-done | bytes 1572896 | tf_op jit(solution)/shard_map/all_to_all | solution.py:42
  97.2 4.5 %copy.22 = bf16[32,192,128]{1,0,2:T(8,128)(2,1)} copy(bf16[32,192,128]{2,1,0:T(8,128)(2,1)} %all-to-all-done.1) | data formatting | bytes 3145728 | tf_op jit(solution)/shard_map/all_to_all | solution.py:42
  101.7 4.5 %reshape.78 = bf16[6144,2,64]{0,2,1:T(8,128)(2,1)} reshape(bf16[32,192,128]{1,0,2:T(8,128)(2,1)} %copy.22) | data formatting | bytes 3145728 | tf_op jit(solution)/shard_map/reshape | solution.py:53
  106.2 2.1 %convolution_convert_fusion = bf16[2,2,64]{2,1,0:T(2,128)(2,1)S(1)} fusion(bf16[6144,2,64]{0,2,1:T(8,128)(2,1)} %reshape.78, f32[2,2,6144]{2,1,0:T(2,128)S(1)} %reduce_window_sum.15, f32[2,2,6144]{2,1,0:T(2,128)S(1)} %get-tuple-element.4), kind=kOutput, calls=%fused_computation.17 | convolution fusion | flops 3588352 | bytes 1769984 | tf_op jit(solution)/shard_map/euq,qec->euc/dot_general | solution.py:63
  108.3 0.7 convert_element_type.48
  108.9 2.7 %copy.40 = bf16[1,6144,128]{2,1,0:T(8,128)(2,1)} copy(bf16[1,6144,128]{2,1,0:T(8,128)(2,1)} %bitcast.5) | data formatting | bytes 3145728
  111.6 2.7 %copy.41 = bf16[1,6144,128]{2,1,0:T(8,128)(2,1)} copy(bf16[1,6144,128]{2,1,0:T(8,128)(2,1)} %bitcast.10) | data formatting | bytes 3145728
  (3 shorter events, 0.0 us)
Async XLA Ops:
  0.6 4.3 %copy-start = (bf16[2048,512]{1,0:T(8,128)(2,1)S(1)}, bf16[2048,512]{1,0:T(8,128)(2,1)}, u32[]{:S(2)}) copy-start(bf16[2048,512]{1,0:T(8,128)(2,1)} %param.8) | copy-start | bytes 6291460
  0.6 5.2 %copy-start.1 = (bf16[8,192,2048]{2,1,0:T(8,128)(2,1)S(1)}, bf16[8,192,2048]{2,1,0:T(8,128)(2,1)}, u32[]{:S(2)}) copy-start(bf16[8,192,2048]{2,1,0:T(8,128)(2,1)} %param.6) | copy-start | bytes 18874372
  0.7 4.3 %copy-start.2 = (bf16[2048]{0:T(1024)(128)(2,1)S(1)}, bf16[2048]{0:T(1024)(128)(2,1)}, u32[]{:S(2)}) copy-start(bf16[2048]{0:T(1024)(128)(2,1)} %param.7) | copy-start | bytes 12292
  10.5 45.1 %all-to-all-start = ((bf16[32,192,128]{2,1,0:T(8,128)(2,1)}), bf16[32,192,128]{2,1,0:T(8,128)(2,1)}, u32[]{:S(2)}, u32[]{:S(2)}) async-start(bf16[32,192,128]{2,1,0:T(8,128)(2,1)} %bitcast.58), calls=%async_computation | async-start | bytes 3145728 | tf_op jit(solution)/shard_map/all_to_all | solution.py:35
  26.1 33.5 %copy-start.3 = (bf16[1,256]{1,0:T(2,128)(2,1)S(1)}, bf16[1,256]{1,0:T(2,128)(2,1)}, u32[]{:S(2)}) copy-start(bf16[1,256]{1,0:T(2,128)(2,1)} %param.10) | copy-start | bytes 1540
  26.1 33.7 %copy-start.4 = (bf16[4]{0:T(256)(128)(2,1)S(1)}, bf16[4]{0:T(256)(128)(2,1)}, u32[]{:S(2)}) copy-start(bf16[4]{0:T(256)(128)(2,1)} %param.11) | copy-start | bytes 28
  55.6 41.6 %all-to-all-start.1 = ((bf16[32,192,128]{2,1,0:T(8,128)(2,1)}), bf16[32,192,128]{2,1,0:T(8,128)(2,1)}, u32[]{:S(2)}, u32[]{:S(2)}) async-start(bf16[32,192,128]{2,1,0:T(8,128)(2,1)} %bitcast.57), calls=%async_computation.1 | async-start | bytes 3145728 | tf_op jit(solution)/shard_map/all_to_all | solution.py:42
where the time goes:
time: 115 us; the launch traced here: 114 us
  waiting for transfers between devices  49.8 us (43%)
  local copies, waits for them, and re-layouts  25.4 us (22%)
  matrix products  16.7 us (15%)
  starting transfers between devices  11.5 us (10%)
  other arithmetic  10.1 us (9%)
    all_to_all x1, waiting for transfers between devices, body(): lax.all_to_all(key_rows.reshape(seq_count * groups, span_len, head_cols),...  29.4 us
    all_to_all x1, waiting for transfers between devices, body(): lax.all_to_all(value_rows.reshape(seq_count * groups, span_len, head_cols...  20.3 us
    dot_general x1, matrix products, body(): jnp.einsum('kru,uao->karo', normed, value_weight.reshape(model_width, gro...  8.19 us
    all_to_all x1, starting transfers between devices, body(): lax.all_to_all(key_rows.reshape(seq_count * groups, span_len, head_cols),...  7.43 us
    unnamed x12, local copies, waits for them, and re-layouts  6.27 us
    another operation x2, other arithmetic  5.69 us
    dot_general x1, matrix products, body(): jnp.einsum('kru,uao->karo', normed, key_weight.reshape(model_width, group...  4.62 us
    all_to_all x1, local copies, waits for them, and re-layouts, body(): lax.all_to_all(key_rows.reshape(seq_count * groups, span_len, head_cols),...  4.53 us
  transfers between devices with their start and end apart: 2, of which 2 were waited for; matrix products, arithmetic and copies ran while one was open for 22% of the time, Pallas kernels for 0%

commit v1 on v0

v1 whole, which is shorter than its diff:
```python
import functools

import jax
import jax.numpy as jnp
from jax import lax
from jax.experimental import pallas as pl
from jax.experimental.pallas import tpu as pltpu
from jax.sharding import PartitionSpec as P

HEAD_DIMENSION = 64
EPSILON = 1e-06
LANES = 128
SUBLANES = 8
MESH = pl.DeviceIdType.MESH


def exchange_kernel(
    n_sp, n_tp, x_hbm, gain_ref, wk_hbm, wv_hbm, land_ref,
    x_buf, w_buf, send_buf, x_sem, w_sem, send_sem, recv_sem,
):
    sp, tp = lax.axis_index("sp"), lax.axis_index("tp")
    me = sp * n_tp + tp
    count = n_sp * n_tp
    span, cols = send_buf.shape[3], send_buf.shape[4]
    half = n_sp // 2

    def sequence_at(i):
        phase = i // half
        block = (sp // half + 1 + phase) % 2
        return block * half + (sp + i + phase) % half

    def x_copy(i):
        return pltpu.make_async_copy(x_hbm.at[sequence_at(i)], x_buf.at[i], x_sem.at[i])

    def w_copy(which):
        source = (wk_hbm, wv_hbm)[which]
        return pltpu.make_async_copy(source, w_buf.at[which], w_sem.at[which])

    x_copy(0).start()
    w_copy(0).start()
    w_copy(1).start()

    barrier = pltpu.get_barrier_semaphore()

    @pl.loop(1, count)
    def _(j):
        other = (me + j) % count
        pl.semaphore_signal(
            barrier, inc=1, device_id=(other // n_tp, other % n_tp), device_id_type=MESH
        )

    @pl.loop(1, n_sp)
    def _(i):
        x_copy(i).start()

    w_copy(0).wait()
    w_copy(1).wait()
    pl.semaphore_wait(barrier, count - 1)

    def send(i, g):
        return pltpu.make_async_remote_copy(
            src_ref=send_buf.at[i, g],
            dst_ref=land_ref.at[:, pl.ds(pl.multiple_of(me * span, span), span), :],
            send_sem=send_sem.at[i, g],
            recv_sem=recv_sem.at[sp, tp],
            device_id=(sequence_at(i), g),
            device_id_type=MESH,
        )

    @pl.loop(0, n_sp)
    def _(i):
        x_copy(i).wait()
        wide = x_buf[i].astype(jnp.float32)
        scale = lax.rsqrt(jnp.mean(wide * wide, axis=-1, keepdims=True) + EPSILON)
        normed = (wide * scale * gain_ref[...].astype(jnp.float32)).astype(jnp.bfloat16)
        for which in range(2):
            rows = jnp.dot(normed, w_buf[which], preferred_element_type=jnp.float32)
            rows = rows.astype(jnp.bfloat16)
            for g in range(n_tp):
                send_buf[i, g, which] = rows[:, g * cols:(g + 1) * cols]
        own = sequence_at(i) == sp
        for j in range(1, n_tp):
            send(i, (tp + j) % n_tp).start()

        @pl.when(jnp.logical_not(own))
        def _():
            send(i, tp).start()

        @pl.when(own)
        def _():
            land_ref[:, pl.ds(pl.multiple_of(me * span, span), span), :] = send_buf[i, tp]

    @pl.loop(1, count)
    def _(j):
        other = (me + j) % count
        pltpu.make_async_remote_copy(
            src_ref=send_buf.at[0, 0],
            dst_ref=land_ref.at[:, pl.ds(pl.multiple_of(other * span, span), span), :],
            send_sem=send_sem.at[0, 0],
            recv_sem=recv_sem.at[other // n_tp, other % n_tp],
            device_id=(sp, tp),
            device_id_type=MESH,
        ).wait_recv()

    @pl.loop(0, n_sp)
    def _(i):
        for j in range(1, n_tp):
            send(i, (tp + j) % n_tp).wait_send()

        @pl.when(sequence_at(i) != sp)
        def _():
            send(i, tp).wait_send()


def read_kernel(repeat, land_ref, query_ref, bias_ref, key_out, value_out, read_ref, sem):
    copies = [
        pltpu.make_async_copy(land_ref.at[0], key_out.at[0], sem.at[0]),
        pltpu.make_async_copy(land_ref.at[1], value_out.at[0], sem.at[1]),
    ]
    for copy in copies:
        copy.start()
    rows = query_ref.shape[0]
    length = land_ref.shape[1]
    chunks = length // LANES
    score = lax.dot_general(
        query_ref[...], land_ref[0], (((1,), (1,)), ((), ())),
        preferred_element_type=jnp.float32,
    )
    score = score + bias_ref[:, 0:1]
    keep = -(jnp.maximum(score, 0.0) + jnp.log1p(jnp.exp(-jnp.abs(score))))
    stacked = jnp.concatenate(
        [keep[:, c * LANES:(c + 1) * LANES] for c in range(chunks)], axis=0
    )
    source = lax.broadcasted_iota(jnp.int32, (LANES, LANES), 0)
    target = lax.broadcasted_iota(jnp.int32, (LANES, LANES), 1)
    later = (source > target).astype(jnp.float32)
    inside = jnp.dot(stacked, later, precision=lax.Precision.HIGHEST)
    total = jnp.dot(stacked, jnp.ones_like(later), precision=lax.Precision.HIGHEST)
    carry = jnp.zeros((rows, LANES), jnp.float32)
    pieces = [None] * chunks
    for c in reversed(range(chunks)):
        pieces[c] = inside[c * rows:(c + 1) * rows] + carry
        carry = carry + total[c * rows:(c + 1) * rows]
    weight = jnp.exp(score + keep + jnp.concatenate(pieces, axis=1)).astype(jnp.bfloat16)
    read = jnp.dot(weight, land_ref[1], preferred_element_type=jnp.float32)
    heads = read_ref.shape[1] // HEAD_DIMENSION
    parts = []
    for h in range(heads):
        left = (h // repeat) * HEAD_DIMENSION
        parts.append(read[h:h + 1, left:left + HEAD_DIMENSION])
    read_ref[...] = jnp.concatenate(parts, axis=1).astype(jnp.bfloat16)
    for copy in copies:
        copy.wait()


def body(n_sp, n_tp, inputs, norm_gain, key_weight, value_weight, query, head_bias):
    seqs, span, width = inputs.shape
    cols = key_weight.shape[1] // n_tp
    kv_heads = cols // HEAD_DIMENSION
    q_heads = query.shape[1] // HEAD_DIMENSION
    repeat = q_heads // kv_heads
    length = span * n_sp * n_tp
    hbm = pl.BlockSpec(memory_space=pl.ANY)
    vmem = pl.BlockSpec(memory_space=pltpu.VMEM)
    landed = pl.pallas_call(
        functools.partial(exchange_kernel, n_sp, n_tp),
        out_shape=jax.ShapeDtypeStruct((2, length, cols), jnp.bfloat16),
        in_specs=[hbm, vmem, hbm, hbm],
        out_specs=vmem,
        scratch_shapes=[
            pltpu.VMEM((seqs, span, width), jnp.bfloat16),
            pltpu.VMEM((2, width, key_weight.shape[1]), jnp.bfloat16),
            pltpu.VMEM((n_sp, n_tp, 2, span, cols), jnp.bfloat16),
            pltpu.SemaphoreType.DMA((n_sp,)),
            pltpu.SemaphoreType.DMA((2,)),
            pltpu.SemaphoreType.DMA((n_sp, n_tp)),
            pltpu.SemaphoreType.DMA((n_sp, n_tp)),
        ],
        compiler_params=pltpu.CompilerParams(
            collective_id=0, has_side_effects=True, vmem_limit_bytes=56 * 2**20
        ),
    )(inputs, norm_gain.reshape(1, width), key_weight, value_weight)

    pad = -q_heads % SUBLANES
    scaled = query.reshape(q_heads, HEAD_DIMENSION) * jnp.bfloat16(HEAD_DIMENSION ** -0.5)
    owner = (jnp.arange(q_heads) // repeat)[:, None] == jnp.arange(kv_heads)[None, :]
    spread = jnp.where(owner[:, :, None], scaled[:, None, :], jnp.bfloat16(0))
    spread = jnp.pad(spread.reshape(q_heads, cols), ((0, pad), (0, 0)))
    bias = jnp.pad(head_bias.astype(jnp.float32), (0, pad))
    bias = jnp.broadcast_to(bias[:, None], (q_heads + pad, LANES))
    return pl.pallas_call(
        functools.partial(read_kernel, repeat),
        out_shape=(
            jax.ShapeDtypeStruct((1, length, cols), jnp.bfloat16),
            jax.ShapeDtypeStruct((1, length, cols), jnp.bfloat16),
            jax.ShapeDtypeStruct((1, q_heads * HEAD_DIMENSION), jnp.bfloat16),
        ),
        in_specs=[vmem, vmem, vmem],
        out_specs=(hbm, hbm, vmem),
        scratch_shapes=[pltpu.SemaphoreType.DMA((2,))],
    )(landed, spread, bias)


def solution(mesh):
    placed = (P(None, ("sp", "tp"), None), P(), P(), P(), P("sp", "tp"), P("tp"))
    return jax.shard_map(
        functools.partial(body, mesh.shape["sp"], mesh.shape["tp"]),
        mesh=mesh,
        in_specs=placed,
        out_specs=(P("sp", None, "tp"), P("sp", None, "tp"), P("sp", "tp")),
        check_vma=False,
    )
```

time: 115 us -> 91.4 us (0.79)
  Pallas kernels: 0 us -> 86.3 us
  waiting for transfers between devices: 49.8 us -> 0 us
  local copies, waits for them, and re-layouts: 25.4 us -> 2.71 us
  matrix products: 16.7 us -> 0 us
  starting transfers between devices: 11.5 us -> 0 us
  other arithmetic: 10.1 us -> 1.52 us
    pallas_call x0 -> x2, Pallas kernels: none -> 86.3 us  [the longest x1 82.1 us: body(): pl.pallas_call(functools.partial(exchange_kernel, n_sp, n_tp), out_shape=...]
    all_to_all x2 -> x0, waiting for transfers between devices: 49.8 us -> none  [the longest x1 29.4 us: body(): lax.all_to_all(key_rows.reshape(seq_count * groups, span_len, head_cols),...]
    dot_general x4 -> x0, matrix products: 16.7 us -> none  [the longest x1 8.19 us: body(): jnp.einsum('kru,uao->karo', normed, value_weight.reshape(model_width, gro...]
    all_to_all x2 -> x0, starting transfers between devices: 11.5 us -> none  [the longest x1 7.43 us: body(): lax.all_to_all(key_rows.reshape(seq_count * groups, span_len, head_cols),...]
    all_to_all x2 -> x0, local copies, waits for them, and re-layouts: 9.06 us -> none  [the longest x1 4.53 us: body(): lax.all_to_all(key_rows.reshape(seq_count * groups, span_len, head_cols),...]
    reshape x4 -> x1, local copies, waits for them, and re-layouts: 9.14 us -> 1.29 us  [body(): norm_gain.reshape(1, width)]
    unnamed x12 -> x0, local copies, waits for them, and re-layouts: 6.27 us -> none
    another operation x3 -> x0, other arithmetic: 5.79 us -> none
  transfers between devices with their start and end apart: 2 -> 0, of which waited for: 2 -> 0; matrix products, arithmetic and copies ran while one was open for 22% -> 0% of each run, Pallas kernels for 0% -> 0%
where the time goes in v1:
time: 91.4 us; the launch traced here: 91.1 us
  Pallas kernels  86.3 us (94%)
  local copies, waits for them, and re-layouts  2.71 us (3%)
  other arithmetic  1.52 us (2%)
    pallas_call x1, Pallas kernels, body(): pl.pallas_call(functools.partial(exchange_kernel, n_sp, n_tp), out_shape=...  82.1 us
    pallas_call x1, Pallas kernels, body(): pl.pallas_call(functools.partial(read_kernel, repeat), out_shape=(jax.Sha...  4.13 us

profile of v1, /device:TPU:0, one launch (start us, length us, event | category | flops | bytes accessed | tf_op | source)
XLA Modules:
  0.0 91.1 jit_solution(362577393731979164)
XLA Ops:
  0.6 0.7 multiply_reduce_fusion
  1.3 0.1 mul.15
  1.4 0.7 pad_convert_fusion
  2.1 0.1 iota_compare_fusion
  2.2 0.1 broadcast_select_fusion
  2.2 0.1 select_n.19
  2.3 0.6 pad.11.query_ref
  2.9 0.7 broadcast_in_dim.33.bias_ref
  3.6 1.3 %reshape.56.gain_ref = bf16[1,2048]{1,0:T(2,128)(2,1)} reshape(bf16[2048]{0:T(1024)(128)(2,1)} %param.7) | data formatting | bytes 8192 | tf_op jit(solution)/shard_map/reshape | solution.py:182
  4.9 82.1 %shard_map.85.land_ref = bf16[2,6144,128]{2,1,0:T(8,128)(2,1)} custom-call(bf16[8,192,2048]{2,1,0:T(8,128)(2,1)} %x_hbm.1, bf16[1,2048]{1,0:T(2,128)(2,1)} %reshape.56.gain_ref, bf16[2048,512]{1,0:T(8,128)(2,1)} %wk_hbm.1, bf16[2048,512]{1,0:T(8,128)(2,1)} %wv_hbm.1), custom_call_target="tpu_custom_call" | custom-call | tf_op jit(solution)/shard_map/pallas_call | solution.py:165
  87.0 4.1 %shard_map.86 = (bf16[1,6144,128]{2,1,0:T(8,128)(2,1)}, bf16[1,6144,128]{2,1,0:T(8,128)(2,1)}, bf16[1,256]{1,0:T(2,128)(2,1)}) custom-call(bf16[2,6144,128]{2,1,0:T(8,128)(2,1)} %shard_map.85.land_ref, bf16[8,128]{1,0:T(8,128)(2,1)} %pad.11.query_ref, f32[8,128]{1,0:T(8,128)} %broadcast_in_dim.33.bias_ref), custom_call_target="tpu_custom_call" | custom-call | tf_op jit(solution)/shard_map/pallas_call | solution.py:191
  (1 shorter events, 0.0 us)

commit v2 on v0

v2 whole, which is shorter than its diff:
```python
import functools

import jax
import jax.numpy as jnp
from jax import lax
from jax.experimental import pallas as pl
from jax.experimental.pallas import tpu as pltpu
from jax.sharding import PartitionSpec as P

HEAD_DIMENSION = 64
EPSILON = 1e-06
LANES = 128
SUBLANES = 8
WRITES = 4
VMEM_BYTES = 67043328
MESH = pl.DeviceIdType.MESH


def group_at(n_sp, sp, i):
    half = n_sp // 2
    block = (sp // half + i // half) % 2
    return block * half + (sp + half - i % half) % half


def spread_query(query_ref, heads, repeat, cols):
    scaled = query_ref[...].astype(jnp.float32) * HEAD_DIMENSION ** -0.5
    rows = []
    for h in range(heads):
        pieces = [jnp.zeros((1, HEAD_DIMENSION), jnp.float32)] * (cols // HEAD_DIMENSION)
        pieces[h // repeat] = scaled[:, h * HEAD_DIMENSION:(h + 1) * HEAD_DIMENSION]
        rows.append(jnp.concatenate(pieces, axis=1))
    rows.append(jnp.zeros((-heads % SUBLANES, cols), jnp.float32))
    return jnp.concatenate(rows, axis=0).astype(jnp.bfloat16)


def bias_column(bias_ref, rows):
    heads = bias_ref.shape[0]
    wide = jnp.broadcast_to(bias_ref[...].astype(jnp.float32).reshape(1, heads), (rows, heads))
    row = lax.broadcasted_iota(jnp.int32, (rows, heads), 0)
    col = lax.broadcasted_iota(jnp.int32, (rows, heads), 1)
    return jnp.sum(jnp.where(row == col, wide, 0.0), axis=1, keepdims=True)


def group_read(spread, bias, keys, values):
    rows = spread.shape[0]
    chunks = keys.shape[0] // LANES
    score = lax.dot_general(
        spread, keys, (((1,), (1,)), ((), ())), preferred_element_type=jnp.float32
    )
    score = score + bias
    keep = -(jnp.maximum(score, 0.0) + jnp.log1p(jnp.exp(-jnp.abs(score))))
    stacked = jnp.concatenate(
        [keep[:, c * LANES:(c + 1) * LANES] for c in range(chunks)], axis=0
    )
    source = lax.broadcasted_iota(jnp.int32, (LANES, LANES), 0)
    target = lax.broadcasted_iota(jnp.int32, (LANES, LANES), 1)
    later = (source > target).astype(jnp.float32)
    inside = jnp.dot(stacked, later, precision=lax.Precision.HIGHEST)
    total = jnp.dot(stacked, jnp.ones_like(later), precision=lax.Precision.HIGHEST)
    carry = jnp.zeros((rows, LANES), jnp.float32)
    pieces = [None] * chunks
    for c in reversed(range(chunks)):
        pieces[c] = inside[c * rows:(c + 1) * rows] + carry
        carry = carry + total[c * rows:(c + 1) * rows]
    weight = jnp.exp(score + keep + jnp.concatenate(pieces, axis=1)).astype(jnp.bfloat16)
    read = jnp.dot(weight, values, preferred_element_type=jnp.float32)
    return read, jnp.broadcast_to(carry[:, 0:1], read.shape)


def exchange_kernel(
    n_sp, n_tp, repeat, x_hbm, gain_hbm, wk_hbm, wv_hbm, query_hbm, bias_hbm,
    land_ref, part_ref, x_buf, w_buf, gain_ref, query_ref, bias_ref, send_buf,
    x_sem, w_sem, small_sem, send_sem, recv_sem,
):
    sp, tp = lax.axis_index("sp"), lax.axis_index("tp")
    me = sp * n_tp + tp
    count = n_sp * n_tp
    span, cols = send_buf.shape[3], send_buf.shape[4]
    half = n_sp // 2
    triples = half // 2

    def sequence_at(i):
        late = i // (3 * triples)
        triple, place = i // 3, i % 3
        near = late + (1 - late) * (place // 2)
        far_offset = 2 * triple + place
        near_offset = triples + late * (i - half) + (1 - late) * triple
        offset = near * near_offset + (1 - near) * far_offset
        return ((sp // half + 1 + near) % 2) * half + (sp + offset) % half

    def x_copy(i):
        return pltpu.make_async_copy(x_hbm.at[sequence_at(i)], x_buf.at[i], x_sem.at[i])

    def w_copy(which):
        source = (wk_hbm, wv_hbm)[which]
        return pltpu.make_async_copy(source, w_buf.at[which], w_sem.at[which])

    small = [
        pltpu.make_async_copy(source, buffer, small_sem.at[k])
        for k, (source, buffer) in enumerate(
            ((gain_hbm, gain_ref), (query_hbm, query_ref), (bias_hbm, bias_ref))
        )
    ]
    barrier = pltpu.get_barrier_semaphore()

    @pl.loop(1, count)
    def _(j):
        other = (me + j) % count
        pl.semaphore_signal(
            barrier, inc=1, device_id=(other // n_tp, other % n_tp), device_id_type=MESH
        )

    small[0].start()
    x_copy(0).start()
    w_copy(0).start()
    w_copy(1).start()
    small[1].start()
    small[2].start()

    @pl.loop(1, n_sp)
    def _(i):
        x_copy(i).start()

    for copy in small:
        copy.wait()
    gain = gain_ref[...].astype(jnp.float32).reshape(1, gain_ref.shape[0])

    def compute(i, first):
        x_copy(i).wait()
        wide = x_buf[i].astype(jnp.float32)
        scale = lax.rsqrt(jnp.mean(wide * wide, axis=-1, keepdims=True) + EPSILON)
        normed = (wide * scale * gain).astype(jnp.bfloat16)
        for which in range(2):
            if first:
                w_copy(which).wait()
            rows = jnp.dot(normed, w_buf[which], preferred_element_type=jnp.float32)
            rows = rows.astype(jnp.bfloat16)
            for g in range(n_tp):
                send_buf[i, g, which] = rows[:, g * cols:(g + 1) * cols]

    def own_rows(source):
        return pl.ds(pl.multiple_of(source * span, span), span)

    def send(i, g):
        return pltpu.make_async_remote_copy(
            src_ref=send_buf.at[i, g],
            dst_ref=land_ref.at[:, own_rows(me), :],
            send_sem=send_sem.at[i, g],
            recv_sem=recv_sem.at[sp, tp],
            device_id=(sequence_at(i), g),
            device_id_type=MESH,
        )

    def send_all(i):
        own = sequence_at(i) == sp
        for j in range(1, n_tp):
            send(i, (tp + j) % n_tp).start()

        @pl.when(jnp.logical_not(own))
        def _():
            send(i, tp).start()

        @pl.when(own)
        def _():
            land_ref[:, own_rows(me), :] = send_buf[i, tp]

    compute(0, True)
    pl.semaphore_wait(barrier, count - 1)
    send_all(0)

    @pl.loop(1, n_sp)
    def _(i):
        compute(i, False)
        send_all(i)

    heads = query_ref.shape[1] // HEAD_DIMENSION
    spread = spread_query(query_ref, heads, repeat, cols)
    bias = bias_column(bias_ref, spread.shape[0])
    group_rows = n_tp * span

    def arrive(source):
        for g in range(n_tp):
            @pl.when(source * n_tp + g != me)
            def _():
                pltpu.make_async_remote_copy(
                    src_ref=send_buf.at[0, 0],
                    dst_ref=land_ref.at[:, own_rows(source * n_tp + g), :],
                    send_sem=send_sem.at[0, 0],
                    recv_sem=recv_sem.at[source, g],
                    device_id=(source, g),
                    device_id_type=MESH,
                ).wait_recv()

    @pl.loop(0, n_sp - 1)
    def _(i):
        source = group_at(n_sp, sp, i)
        arrive(source)
        at = pl.ds(pl.multiple_of(source * group_rows, group_rows), group_rows)
        read, total = group_read(spread, bias, land_ref[0, at, :], land_ref[1, at, :])
        part_ref[source, 0] = read
        part_ref[source, 1] = total

    part_ref[n_sp, 0] = spread.astype(jnp.float32)
    part_ref[n_sp, 1] = jnp.broadcast_to(bias, spread.shape)
    last = group_at(n_sp, sp, n_sp - 1)
    part_ref[last] = jnp.zeros(part_ref.shape[1:], jnp.float32)

    @pl.loop(0, n_sp)
    def _(i):
        for j in range(1, n_tp):
            send(i, (tp + j) % n_tp).wait_send()

        @pl.when(sequence_at(i) != sp)
        def _():
            send(i, tp).wait_send()

    arrive(last)


def write_kernel(
    n_sp, repeat, land_ref, part_ref, key_out, value_out, read_ref, part, sem
):
    length, cols = land_ref.shape[1:]
    copies = []
    for which, out in enumerate((key_out, value_out)):
        for c in range(WRITES):
            at = pl.ds(c * (length // WRITES), length // WRITES)
            copies.append(
                pltpu.make_async_copy(land_ref.at[which, at], out.at[0, at], sem.at[which, c])
            )
    for copy in copies:
        copy.start()
    heads = read_ref.shape[1] // HEAD_DIMENSION
    group_rows = length // n_sp
    spread = part_ref[n_sp, 0].astype(jnp.bfloat16)
    bias = part_ref[n_sp, 1][:, 0:1]
    last = group_at(n_sp, lax.axis_index("sp"), n_sp - 1)
    at = pl.ds(pl.multiple_of(last * group_rows, group_rows), group_rows)
    read, total = group_read(spread, bias, land_ref[0, at, :], land_ref[1, at, :])
    part[...] = part_ref[0:n_sp]
    part[last, 0] = read
    part[last, 1] = total
    after = jnp.zeros_like(total)
    whole = jnp.zeros_like(read)
    for p in reversed(range(n_sp)):
        whole = whole + jnp.exp(after) * part[p, 0]
        after = after + part[p, 1]
    pieces = []
    for h in range(heads):
        left = (h // repeat) * HEAD_DIMENSION
        pieces.append(whole[h:h + 1, left:left + HEAD_DIMENSION])
    read_ref[...] = jnp.concatenate(pieces, axis=1).astype(jnp.bfloat16)
    for copy in copies:
        copy.wait()


def body(n_sp, n_tp, inputs, norm_gain, key_weight, value_weight, query, head_bias):
    seqs, span, width = inputs.shape
    cols = key_weight.shape[1] // n_tp
    q_heads = query.shape[1] // HEAD_DIMENSION
    repeat = q_heads // (cols // HEAD_DIMENSION)
    length = span * n_sp * n_tp
    rows = q_heads + -q_heads % SUBLANES
    lanes = cols + -cols % LANES
    kept = 2 * length * lanes * 2 + (n_sp + 1) * 2 * rows * lanes * 4
    hbm = pl.BlockSpec(memory_space=pltpu.HBM)
    vmem = pl.BlockSpec(memory_space=pltpu.VMEM)
    landed, parts = pl.pallas_call(
        functools.partial(exchange_kernel, n_sp, n_tp, repeat),
        out_shape=(
            pltpu.VMEM((2, length, cols), jnp.bfloat16),
            pltpu.VMEM((n_sp + 1, 2, rows, cols), jnp.float32),
        ),
        in_specs=[hbm] * 6,
        out_specs=(vmem, vmem),
        scratch_shapes=[
            pltpu.VMEM((seqs, span, width), jnp.bfloat16),
            pltpu.VMEM((2, width, key_weight.shape[1]), jnp.bfloat16),
            pltpu.VMEM(norm_gain.shape, norm_gain.dtype),
            pltpu.VMEM(query.shape, query.dtype),
            pltpu.VMEM(head_bias.shape, head_bias.dtype),
            pltpu.VMEM((n_sp, n_tp, 2, span, cols), jnp.bfloat16),
            pltpu.SemaphoreType.DMA((n_sp,)),
            pltpu.SemaphoreType.DMA((2,)),
            pltpu.SemaphoreType.DMA((3,)),
            pltpu.SemaphoreType.DMA((n_sp, n_tp)),
            pltpu.SemaphoreType.DMA((n_sp, n_tp)),
        ],
        compiler_params=pltpu.CompilerParams(
            collective_id=0, has_side_effects=True, vmem_limit_bytes=VMEM_BYTES - kept
        ),
    )(inputs, norm_gain, key_weight, value_weight, query, head_bias)
    return pl.pallas_call(
        functools.partial(write_kernel, n_sp, repeat),
        out_shape=(
            jax.ShapeDtypeStruct((1, length, cols), jnp.bfloat16),
            jax.ShapeDtypeStruct((1, length, cols), jnp.bfloat16),
            jax.ShapeDtypeStruct((1, q_heads * HEAD_DIMENSION), jnp.bfloat16),
        ),
        in_specs=[vmem, vmem],
        out_specs=(hbm, hbm, vmem),
        scratch_shapes=[
            pltpu.VMEM((n_sp, 2, rows, cols), jnp.float32),
            pltpu.SemaphoreType.DMA((2, WRITES)),
        ],
        compiler_params=pltpu.CompilerParams(vmem_limit_bytes=16 * 2**20),
    )(landed, parts)


def solution(mesh):
    placed = (P(None, ("sp", "tp"), None), P(), P(), P(), P("sp", "tp"), P("tp"))
    return jax.shard_map(
        functools.partial(body, mesh.shape["sp"], mesh.shape["tp"]),
        mesh=mesh,
        in_specs=placed,
        out_specs=(P("sp", None, "tp"), P("sp", None, "tp"), P("sp", "tp")),
        check_vma=False,
    )
```

time: 115 us -> 90.7 us (0.79)
  Pallas kernels: 0 us -> 89.8 us
  waiting for transfers between devices: 49.8 us -> 0 us
  local copies, waits for them, and re-layouts: 25.4 us -> 0 us
  matrix products: 16.7 us -> 0 us
  starting transfers between devices: 11.5 us -> 0 us
  other arithmetic: 10.1 us -> 0 us
    pallas_call x0 -> x2, Pallas kernels: none -> 89.8 us  [the longest x1 87.4 us: body(): pl.pallas_call(functools.partial(exchange_kernel, n_sp, n_tp, repeat), ou...]
    all_to_all x2 -> x0, waiting for transfers between devices: 49.8 us -> none  [the longest x1 29.4 us: body(): lax.all_to_all(key_rows.reshape(seq_count * groups, span_len, head_cols),...]
    dot_general x4 -> x0, matrix products: 16.7 us -> none  [the longest x1 8.19 us: body(): jnp.einsum('kru,uao->karo', normed, value_weight.reshape(model_width, gro...]
    all_to_all x2 -> x0, starting transfers between devices: 11.5 us -> none  [the longest x1 7.43 us: body(): lax.all_to_all(key_rows.reshape(seq_count * groups, span_len, head_cols),...]
    reshape x4 -> x0, local copies, waits for them, and re-layouts: 9.14 us -> none  [the longest x1 4.49 us: body(): key_tensor = key_cache.reshape(seq_len, kv_heads, HEAD_DIMENSION)]
    all_to_all x2 -> x0, local copies, waits for them, and re-layouts: 9.06 us -> none  [the longest x1 4.53 us: body(): lax.all_to_all(key_rows.reshape(seq_count * groups, span_len, head_cols),...]
    unnamed x12 -> x0, local copies, waits for them, and re-layouts: 6.27 us -> none
    another operation x3 -> x0, other arithmetic: 5.79 us -> none
  transfers between devices with their start and end apart: 2 -> 0, of which waited for: 2 -> 0; matrix products, arithmetic and copies ran while one was open for 22% -> 0% of each run, Pallas kernels for 0% -> 0%
where the time goes in v2:
time: 90.7 us; the launch traced here: 90.5 us
  Pallas kernels  89.8 us (99%)
    pallas_call x1, Pallas kernels, body(): pl.pallas_call(functools.partial(exchange_kernel, n_sp, n_tp, repeat), ou...  87.4 us
    pallas_call x1, Pallas kernels, body(): pl.pallas_call(functools.partial(write_kernel, n_sp, repeat), out_shape=(...  2.47 us

profile of v2, /device:TPU:0, one launch (start us, length us, event | category | flops | bytes accessed | tf_op | source)
XLA Modules:
  0.0 90.5 jit_solution(17507589024394386075)
XLA Ops:
  0.6 87.4 %shard_map.85 = (bf16[2,6144,128]{2,1,0:T(8,128)(2,1)S(1)}, f32[9,2,8,128]{3,2,1,0:T(8,128)S(1)}) custom-call(bf16[8,192,2048]{2,1,0:T(8,128)(2,1)} %x_hbm.1, bf16[2048]{0:T(1024)(128)(2,1)} %gain_hbm.1, bf16[2048,512]{1,0:T(8,128)(2,1)} %wk_hbm.1, bf16[2048,512]{1,0:T(8,128)(2,1)} %wv_hbm.1, bf16[1,256]{1,0:T(2,128)(2,1)} %query_hbm.1, bf16[4]{0:T(256)(128)(2,1)} %bias_hbm.1), custom_call_target="tpu_custom_call" | custom-call | tf_op jit(solution)/shard_map/pallas_call | solution.py:268
  88.0 2.5 %shard_map.86 = (bf16[1,6144,128]{2,1,0:T(8,128)(2,1)}, bf16[1,6144,128]{2,1,0:T(8,128)(2,1)}, bf16[1,256]{1,0:T(2,128)(2,1)}) custom-call(bf16[2,6144,128]{2,1,0:T(8,128)(2,1)S(1)} %get-tuple-element.5.land_ref, f32[9,2,8,128]{3,2,1,0:T(8,128)S(1)} %get-tuple-element.6.part_ref), custom_call_target="tpu_custom_call" | custom-call | tf_op jit(solution)/shard_map/pallas_call | solution.py:293

commit v3 on v2

--- a/solution.py
+++ b/solution.py
@@ -16,10 +16,31 @@
 MESH = pl.DeviceIdType.MESH
 
 
-def group_at(n_sp, sp, i):
+def flip(index, mask, size):
+    bits = [1 << b for b in range((size - 1).bit_length())]
+    return sum(((index // bit + mask // bit) % 2) * bit for bit in bits)
+
+
+def far_mask(half, a):
+    return half + (a % 2) * (half // 2) + a // 2
+
+
+def send_mask(n_sp, i):
     half = n_sp // 2
-    block = (sp // half + i // half) % 2
-    return block * half + (sp + half - i % half) % half
+    quarter = half // 2
+    late = i // (3 * quarter)
+    triple, place = i // 3, i % 3
+    near = late + (1 - late) * (place // 2)
+    q = late * (i - half) + (1 - late) * triple
+    second = q // quarter
+    near_mask = (1 - second) * (quarter + q) + second * (half - 1 - q)
+    return near * near_mask + (1 - near) * far_mask(half, 2 * triple + place)
+
+
+def read_mask(n_sp, i):
+    half = n_sp // 2
+    late = i // half
+    return (1 - late) * i + late * far_mask(half, i - half)
 
 
 def spread_query(query_ref, heads, repeat, cols):
@@ -76,17 +97,9 @@
     me = sp * n_tp + tp
     count = n_sp * n_tp
     span, cols = send_buf.shape[3], send_buf.shape[4]
-    half = n_sp // 2
-    triples = half // 2
 
     def sequence_at(i):
-        late = i // (3 * triples)
-        triple, place = i // 3, i % 3
-        near = late + (1 - late) * (place // 2)
-        far_offset = 2 * triple + place
-        near_offset = triples + late * (i - half) + (1 - late) * triple
-        offset = near * near_offset + (1 - near) * far_offset
-        return ((sp // half + 1 + near) % 2) * half + (sp + offset) % half
+        return flip(sp, send_mask(n_sp, i), n_sp)
 
     def x_copy(i):
         return pltpu.make_async_copy(x_hbm.at[sequence_at(i)], x_buf.at[i], x_sem.at[i])
@@ -154,7 +167,7 @@
     def send_all(i):
         own = sequence_at(i) == sp
         for j in range(1, n_tp):
-            send(i, (tp + j) % n_tp).start()
+            send(i, flip(tp, j, n_tp)).start()
 
         @pl.when(jnp.logical_not(own))
         def _():
@@ -193,7 +206,7 @@
 
     @pl.loop(0, n_sp - 1)
     def _(i):
-        source = group_at(n_sp, sp, i)
+        source = flip(sp, read_mask(n_sp, i), n_sp)
         arrive(source)
         at = pl.ds(pl.multiple_of(source * group_rows, group_rows), group_rows)
         read, total = group_read(spread, bias, land_ref[0, at, :], land_ref[1, at, :])
@@ -202,13 +215,13 @@
 
     part_ref[n_sp, 0] = spread.astype(jnp.float32)
     part_ref[n_sp, 1] = jnp.broadcast_to(bias, spread.shape)
-    last = group_at(n_sp, sp, n_sp - 1)
+    last = flip(sp, n_sp - 1, n_sp)
     part_ref[last] = jnp.zeros(part_ref.shape[1:], jnp.float32)
 
     @pl.loop(0, n_sp)
     def _(i):
         for j in range(1, n_tp):
-            send(i, (tp + j) % n_tp).wait_send()
+            send(i, flip(tp, j, n_tp)).wait_send()
 
         @pl.when(sequence_at(i) != sp)
         def _():
@@ -234,7 +247,7 @@
     group_rows = length // n_sp
     spread = part_ref[n_sp, 0].astype(jnp.bfloat16)
     bias = part_ref[n_sp, 1][:, 0:1]
-    last = group_at(n_sp, lax.axis_index("sp"), n_sp - 1)
+    last = flip(lax.axis_index("sp"), n_sp - 1, n_sp)
     at = pl.ds(pl.multiple_of(last * group_rows, group_rows), group_rows)
     read, total = group_read(spread, bias, land_ref[0, at, :], land_ref[1, at, :])
     part[...] = part_ref[0:n_sp]

time: 90.7 us -> 82.2 us (0.906)
  the two profiles are of different devices: /device:TPU:0 before, /device:TPU:8 now
where the time goes in v3:
time: 82.2 us; the launch traced here: 82 us
  Pallas kernels  81.3 us (99%)
    pallas_call x1, Pallas kernels, body(): pl.pallas_call(functools.partial(exchange_kernel, n_sp, n_tp, repeat), ou...  78.9 us
    pallas_call x1, Pallas kernels, body(): pl.pallas_call(functools.partial(write_kernel, n_sp, repeat), out_shape=(...  2.47 us

profile of v3, /device:TPU:8, one launch (start us, length us, event | category | flops | bytes accessed | tf_op | source)
XLA Modules:
  0.0 82.0 jit_solution(18404546342798152008)
XLA Ops:
  0.6 78.9 %shard_map.85 = (bf16[2,6144,128]{2,1,0:T(8,128)(2,1)S(1)}, f32[9,2,8,128]{3,2,1,0:T(8,128)S(1)}) custom-call(bf16[8,192,2048]{2,1,0:T(8,128)(2,1)} %x_hbm.1, bf16[2048]{0:T(1024)(128)(2,1)} %gain_hbm.1, bf16[2048,512]{1,0:T(8,128)(2,1)} %wk_hbm.1, bf16[2048,512]{1,0:T(8,128)(2,1)} %wv_hbm.1, bf16[1,256]{1,0:T(2,128)(2,1)} %query_hbm.1, bf16[4]{0:T(256)(128)(2,1)} %bias_hbm.1), custom_call_target="tpu_custom_call" | custom-call | tf_op jit(solution)/shard_map/pallas_call | solution.py:281
  79.5 2.5 %shard_map.86 = (bf16[1,6144,128]{2,1,0:T(8,128)(2,1)}, bf16[1,6144,128]{2,1,0:T(8,128)(2,1)}, bf16[1,256]{1,0:T(2,128)(2,1)}) custom-call(bf16[2,6144,128]{2,1,0:T(8,128)(2,1)S(1)} %get-tuple-element.5.land_ref, f32[9,2,8,128]{3,2,1,0:T(8,128)S(1)} %get-tuple-element.6.part_ref), custom_call_target="tpu_custom_call" | custom-call | tf_op jit(solution)/shard_map/pallas_call | solution.py:306

commit v4 on v3

--- a/solution.py
+++ b/solution.py
@@ -164,10 +164,11 @@
             device_id_type=MESH,
         )
 
-    def send_all(i):
+    def send_one(i, j):
+        if j:
+            send(i, flip(tp, j, n_tp)).start()
+            return
         own = sequence_at(i) == sp
-        for j in range(1, n_tp):
-            send(i, flip(tp, j, n_tp)).start()
 
         @pl.when(jnp.logical_not(own))
         def _():
@@ -177,14 +178,23 @@
         def _():
             land_ref[:, own_rows(me), :] = send_buf[i, tp]
 
+    turns = list(range(1, n_tp)) + [0]
+    now, later = turns[:n_tp // 2], turns[n_tp // 2:]
+
     compute(0, True)
     pl.semaphore_wait(barrier, count - 1)
-    send_all(0)
+    for j in now:
+        send_one(0, j)
 
     @pl.loop(1, n_sp)
     def _(i):
         compute(i, False)
-        send_all(i)
+        for j, k in zip(now, later):
+            send_one(i, j)
+            send_one(i - 1, k)
+
+    for k in later:
+        send_one(n_sp - 1, k)
 
     heads = query_ref.shape[1] // HEAD_DIMENSION
     spread = spread_query(query_ref, heads, repeat, cols)

time: 82.2 us -> 79.9 us (0.972)
  the two profiles are of different devices: /device:TPU:8 before, /device:TPU:0 now
where the time goes in v4:
time: 79.9 us; the launch traced here: 79.3 us
  Pallas kernels  78.6 us (98%)
    pallas_call x1, Pallas kernels, body(): pl.pallas_call(functools.partial(exchange_kernel, n_sp, n_tp, repeat), ou...  76.2 us
    pallas_call x1, Pallas kernels, body(): pl.pallas_call(functools.partial(write_kernel, n_sp, repeat), out_shape=(...  2.47 us

profile of v4, /device:TPU:0, one launch (start us, length us, event | category | flops | bytes accessed | tf_op | source)
XLA Modules:
  0.0 79.3 jit_solution(3703802482665310583)
XLA Ops:
  0.6 76.2 %shard_map.85 = (bf16[2,6144,128]{2,1,0:T(8,128)(2,1)S(1)}, f32[9,2,8,128]{3,2,1,0:T(8,128)S(1)}) custom-call(bf16[8,192,2048]{2,1,0:T(8,128)(2,1)} %x_hbm.1, bf16[2048]{0:T(1024)(128)(2,1)} %gain_hbm.1, bf16[2048,512]{1,0:T(8,128)(2,1)} %wk_hbm.1, bf16[2048,512]{1,0:T(8,128)(2,1)} %wv_hbm.1, bf16[1,256]{1,0:T(2,128)(2,1)} %query_hbm.1, bf16[4]{0:T(256)(128)(2,1)} %bias_hbm.1), custom_call_target="tpu_custom_call" | custom-call | tf_op jit(solution)/shard_map/pallas_call | solution.py:291
  76.8 2.5 %shard_map.86 = (bf16[1,6144,128]{2,1,0:T(8,128)(2,1)}, bf16[1,6144,128]{2,1,0:T(8,128)(2,1)}, bf16[1,256]{1,0:T(2,128)(2,1)}) custom-call(bf16[2,6144,128]{2,1,0:T(8,128)(2,1)S(1)} %get-tuple-element.5.land_ref, f32[9,2,8,128]{3,2,1,0:T(8,128)S(1)} %get-tuple-element.6.part_ref), custom_call_target="tpu_custom_call" | custom-call | tf_op jit(solution)/shard_map/pallas_call | solution.py:316
